TPU v7x, 32 devices: a whole 2x2x4 slice. The times are simulated.
32 devices in a mesh: tp: 16 (over z, y, core), dp: 2 (over x).
Axes of the slice: x: 2, y: 2, z: 4, core: 2. Of those that a mesh axis runs over, the one named last changes fastest.
Arguments:
- resid: bfloat16 [64, 2048], P('dp', 'tp'), may hold values from -6 to 6
- norm_gain: float32 [2, 2048], replicated, may hold values from 0.1 to 1.9
- w_query: bfloat16 [2, 2048, 2048], P(None, 'dp', 'tp'), may hold values from -0.125 to 0.125
- w_forget: bfloat16 [2, 2048, 2048], P(None, 'dp', 'tp'), may hold values from -0.125 to 0.125
- w_value: bfloat16 [2, 2048, 16, 128], P(None, 'dp', None, 'tp'), may hold values from -0.125 to 0.125
- w_gate: bfloat16 [2, 2048, 16, 128], P(None, 'dp', None, 'tp'), may hold values from -0.125 to 0.125
- gate_floor: float32 [2, 2048], replicated, may hold values from 0 to 0.9
- states: float32 [2, 64, 16, 128, 128], P(None, 'dp', None, 'tp'), may hold values from -1 to 1
- out_gain: float32 [2, 16, 128], P(None, None, 'tp'), may hold values from 0.1 to 1.9
- w_out: bfloat16 [2, 16, 128, 2048], P(None, None, 'tp'), may hold values from -0.125 to 0.125
Outputs:
- new_resid: bfloat16 [64, 2048], P('dp', 'tp')
- new_states: float32 [2, 64, 16, 128, 128], P(None, 'dp', None, 'tp')
All inputs are finite; a program needn't handle non-finite values.
Results may differ from a plain program's by a relative error of at most 0.029.
Values may be sent and summed in bfloat16 or wider, within the bound.
No kernel may reach another device: no remote copies, remote signals or barrier semaphores. Data moves between devices by JAX's collectives and lax.ppermute only.
A program may use at most 64 MiB of HBM per device.

v0:
```python
import jax
import jax.numpy as jnp
from jax import lax
from jax.sharding import PartitionSpec as P

BLOCKS = 2


epsilon = 1e-06


def shards(
    resid, norm_gain, w_query, w_forget, w_value, w_gate, gate_floor, states, out_gain, w_out
):
    residual = resid
    seq_local = resid.shape[0]
    heads = states.shape[2]
    slice_cols = states.shape[3]
    head_dim = states.shape[4]
    row_count = w_query.shape[1]
    new_list = []
    for layer in range(BLOCKS):
        gathered = lax.all_gather(residual, "tp", axis=1, tiled=True)
        resid_f32 = gathered.astype(jnp.float32)
        inv_rms = lax.rsqrt(jnp.mean(resid_f32 * resid_f32, axis=1, keepdims=True) + epsilon)
        scaled = (resid_f32 * norm_gain[layer]).astype(jnp.bfloat16)
        query_rows = w_query[layer]
        forget_rows = w_forget[layer]
        value_rows = w_value[layer].reshape(row_count, -1)
        gate_rows = w_gate[layer].reshape(row_count, -1)
        zero_sums = (
            jnp.zeros((seq_local, query_rows.shape[1]), jnp.float32),
            jnp.zeros((seq_local, forget_rows.shape[1]), jnp.float32),
            jnp.zeros((seq_local, value_rows.shape[1]), jnp.float32),
            jnp.zeros((seq_local, gate_rows.shape[1]), jnp.float32),
        )
        totals = zero_sums
        pieces = (
            lax.all_gather(query_rows, "dp", axis=0, tiled=True),
            lax.all_gather(forget_rows, "dp", axis=0, tiled=True),
            lax.all_gather(value_rows, "dp", axis=0, tiled=True),
            lax.all_gather(gate_rows, "dp", axis=0, tiled=True),
        )
        segments = pieces[0].shape[0] // row_count
        for part_index in range(segments):
            columns = lax.dynamic_slice_in_dim(scaled, part_index * row_count, row_count, 1)
            lo_row = part_index * row_count
            totals = tuple(
                (
                    total
                    + lax.optimization_barrier(
                        jnp.dot(
                            columns,
                            segment[lo_row : lo_row + row_count],
                            preferred_element_type=jnp.float32,
                        ).astype(jnp.bfloat16)
                    ).astype(jnp.float32)
                    for total, segment in zip(totals, pieces)
                )
            )
        queries, forget_pre, values, gate_pre = [
            (summed * inv_rms).astype(jnp.bfloat16) for summed in totals
        ]
        query_all, forget_all = (
            lax.all_gather(queries, "tp", axis=1, tiled=True),
            lax.all_gather(forget_pre, "tp", axis=1, tiled=True),
        )
        floor_now = gate_floor[layer]
        keep = floor_now + (1.0 - floor_now) * jax.nn.sigmoid(forget_all.astype(jnp.float32))
        keep = keep.reshape(seq_local, heads, head_dim)
        value_f32 = values.astype(jnp.float32).reshape(seq_local, heads, slice_cols)
        state_new = (
            keep[:, :, None, :] * states[layer]
            + (1.0 - keep)[:, :, None, :] * value_f32[:, :, :, None]
        )
        query_f32 = query_all.astype(jnp.float32).reshape(seq_local, heads, head_dim)
        readout = jnp.sum(query_f32[:, :, None, :] * state_new, axis=3)
        power_sum = lax.psum(jnp.sum(readout * readout, axis=2), "tp")
        mean_square = power_sum[..., None] / head_dim
        gate_f32 = gate_pre.astype(jnp.float32).reshape(seq_local, heads, slice_cols)
        normed = (
            readout * lax.rsqrt(mean_square + epsilon) * out_gain[layer] * jax.nn.silu(gate_f32)
        ).astype(jnp.bfloat16)
        flattened = normed.reshape(seq_local, heads * slice_cols)
        weight_out = w_out[layer].reshape(heads * slice_cols, -1)
        branch = lax.psum_scatter(
            lax.dot_general(
                weight_out, flattened, (((0,), (1,)), ((), ())), preferred_element_type=jnp.float32
            ),
            "tp",
            scatter_dimension=0,
            tiled=True,
        )
        residual = (residual.astype(jnp.float32) + branch.T).astype(jnp.bfloat16)
        new_list.append(state_new)
    return (residual, jnp.stack(new_list))


def solution(mesh):
    return jax.shard_map(
        shards,
        mesh=mesh,
        in_specs=(
            P("dp", "tp"),
            P(),
            P(None, "dp", "tp"),
            P(None, "dp", "tp"),
            P(None, "dp", None, "tp"),
            P(None, "dp", None, "tp"),
            P(),
            P(None, "dp", None, "tp", None),
            P(None, None, "tp"),
            P(None, None, "tp", None),
        ),
        out_specs=(P("dp", "tp"), P(None, "dp", None, "tp", None)),
        check_vma=False,
    )
```

profile of v0, /device:TPU:0, one launch (start us, length us, event | category | flops | bytes accessed | tf_op | source)
XLA Modules:
  0.0 405.7 jit_solution(406525206643660046)
XLA Ops:
  7.2 0.8 fusion.65
  8.0 23.7 %all_gather.42 = bf16[32,2048]{1,0:T(8,128)(2,1)S(1)} all-gather(bf16[32,128]{1,0:T(8,128)(2,1)} %param.10), channel_id=1, replica_groups=mesh['tp'=16,'dp'=2] {'tp'}, dimensions={1}, use_global_device_ids=true | all-gather | bytes 139264 | tf_op jit(solution)/shard_map/all_gather | solution.py:23
  31.8 1.1 fusion.62
  32.8 9.4 %all-gather = bf16[1,2048,128]{2,1,0:T(8,128)(2,1)S(1)} all-gather(bf16[1,1024,128]{2,1,0:T(8,128)(2,1)S(1)} %get-tuple-element.7), channel_id=2, replica_groups=mesh['tp'=16,'dp'=2] {'dp'}, dimensions={1}, use_global_device_ids=true | all-gather | bytes 786432 | tf_op jit(solution)/shard_map/all_gather | solution.py:39
  42.2 0.1 fusion.11
  42.3 0.2 convolution_convert_fusion.15
  42.5 0.2 convolution_convert_fusion.14
  42.7 8.5 %all-gather.1 = bf16[1,2048,128]{2,1,0:T(8,128)(2,1)S(1)} all-gather(bf16[1,1024,128]{2,1,0:T(8,128)(2,1)S(1)} %get-tuple-element.9), channel_id=3, replica_groups=mesh['tp'=16,'dp'=2] {'dp'}, dimensions={1}, use_global_device_ids=true | all-gather | bytes 786432 | tf_op jit(solution)/shard_map/all_gather | solution.py:40
  51.2 0.2 convolution_convert_fusion.13
  51.4 0.2 convolution_convert_fusion.12
  51.7 7.5 %all_gather.47 = bf16[2048,128]{0,1:T(8,128)(2,1)S(1)} all-gather(bf16[1024,128]{0,1:T(8,128)(2,1)S(1)} %get-tuple-element.10), channel_id=1, replica_groups=mesh['tp'=16,'dp'=2] {'dp'}, dimensions={0}, use_global_device_ids=true | all-gather | bytes 786432 | tf_op jit(solution)/shard_map/all_gather | solution.py:41
  59.2 0.2 convolution_convert_fusion.10
  59.3 0.2 convolution_convert_fusion.11
  59.6 7.0 %all_gather.48 = bf16[2048,128]{0,1:T(8,128)(2,1)S(1)} all-gather(bf16[1024,128]{0,1:T(8,128)(2,1)S(1)} %get-tuple-element.5), channel_id=1, replica_groups=mesh['tp'=16,'dp'=2] {'dp'}, dimensions={0}, use_global_device_ids=true | all-gather | bytes 786432 | tf_op jit(solution)/shard_map/all_gather | solution.py:42
  66.6 0.2 convolution_convert_fusion.8
  66.8 0.2 convolution_convert_fusion.9
  67.1 0.1 copy.27
  67.1 0.1 mul.312
  67.3 0.1 multiply_convert_fusion.7
  67.4 0.1 copy.24
  67.5 17.5 %all_gather.44 = bf16[32,2048]{1,0:T(8,128)(2,1)S(1)} all-gather(bf16[32,128]{1,0:T(8,128)(2,1)S(1)} %get-tuple-element.27), channel_id=1, replica_groups=mesh['tp'=16,'dp'=2] {'tp'}, dimensions={1}, use_global_device_ids=true | all-gather | bytes 139264 | tf_op jit(solution)/shard_map/all_gather | solution.py:65
  85.0 19.4 %all_gather.46 = bf16[32,2048]{1,0:T(8,128)(2,1)S(1)} all-gather(bf16[32,128]{1,0:T(8,128)(2,1)S(1)} %get-tuple-element.28), channel_id=1, replica_groups=mesh['tp'=16,'dp'=2] {'tp'}, dimensions={1}, use_global_device_ids=true | all-gather | bytes 139264 | tf_op jit(solution)/shard_map/all_gather | solution.py:66
  104.4 0.1 add_bitcast_fusion.1
  104.6 0.2 copy.25
  104.8 2.6 fusion.5
  107.4 0.1 multiply_reduce_fusion.1
  107.6 57.8 %psum.14 = f32[32,16]{1,0:T(8,128)S(1)} all-reduce(f32[32,16]{1,0:T(8,128)S(1)} %multiply_reduce_fusion.1), channel_id=1, replica_groups=mesh['tp'=16,'dp'=2] {'tp'}, use_global_device_ids=true, to_apply=%region_3.0 | all-reduce | flops 512 | bytes 4096 | tf_op jit(solution)/shard_map/psum | solution.py:78
  165.4 0.1 broadcast_multiply_fusion.1
  165.6 0.2 copy.26
  165.8 1.0 convolution_bitcast_fusion.1
  166.9 0.1 copy.32
  166.9 0.1 mul.345
  167.0 9.5 %all-gather.2 = bf16[1,2048,128]{2,1,0:T(8,128)(2,1)} all-gather(bf16[1,1024,128]{2,1,0:T(8,128)(2,1)S(1)} %get-tuple-element.6), channel_id=4, replica_groups=mesh['tp'=16,'dp'=2] {'dp'}, dimensions={1}, use_global_device_ids=true | all-gather | bytes 786432 | tf_op jit(solution)/shard_map/all_gather | solution.py:39
  176.5 9.2 %all-gather.3 = bf16[1,2048,128]{2,1,0:T(8,128)(2,1)S(1)} all-gather(bf16[1,1024,128]{2,1,0:T(8,128)(2,1)S(1)} %get-tuple-element.8), channel_id=5, replica_groups=mesh['tp'=16,'dp'=2] {'dp'}, dimensions={1}, use_global_device_ids=true | all-gather | bytes 786432 | tf_op jit(solution)/shard_map/all_gather | solution.py:40
  185.7 8.4 %all_gather.54 = bf16[2048,128]{0,1:T(8,128)(2,1)} all-gather(bf16[1024,128]{0,1:T(8,128)(2,1)S(1)} %get-tuple-element.11), channel_id=1, replica_groups=mesh['tp'=16,'dp'=2] {'dp'}, dimensions={0}, use_global_device_ids=true | all-gather | bytes 786432 | tf_op jit(solution)/shard_map/all_gather | solution.py:41
  194.1 7.1 %all_gather.55 = bf16[2048,128]{0,1:T(8,128)(2,1)} all-gather(bf16[1024,128]{0,1:T(8,128)(2,1)S(1)} %get-tuple-element.4), channel_id=1, replica_groups=mesh['tp'=16,'dp'=2] {'dp'}, dimensions={0}, use_global_device_ids=true | all-gather | bytes 786432 | tf_op jit(solution)/shard_map/all_gather | solution.py:42
  201.3 18.7 %reduce-scatter.3.cloned.1.call-done = f32[128,32]{0,1:T(8,128)} async-done(((f32[2048,32]{0,1:T(8,128)}), f32[128,32]{0,1:T(8,128)}) %reduce-scatter.3.cloned.1.call-update) | async-done | bytes 16400 | tf_op jit(solution)/shard_map/reduce_scatter | solution.py:86
  220.0 0.7 fusion.47
  220.7 19.7 %all_gather.49 = bf16[32,2048]{1,0:T(8,128)(2,1)S(1)} all-gather(bf16[32,128]{1,0:T(8,128)(2,1)S(1)} %fusion.47), channel_id=1, replica_groups=mesh['tp'=16,'dp'=2] {'tp'}, dimensions={1}, use_global_device_ids=true | all-gather | bytes 139264 | tf_op jit(solution)/shard_map/all_gather | solution.py:23
  240.4 0.2 fusion.13
  240.6 0.2 convolution_convert_fusion.5
  240.8 0.2 convolution_convert_fusion.4
  240.9 1.1 convolution_convert_fusion.3
  242.1 1.2 convolution_convert_fusion.2
  243.2 1.2 convolution_convert_fusion.1
  244.4 0.2 convolution_convert_fusion
  244.6 0.2 convolution_convert_fusion.6
  244.8 0.2 convolution_convert_fusion.7
  245.0 0.1 multiply_convert_fusion.3
  245.1 0.1 copy.29
  245.2 17.8 %all_gather.51 = bf16[32,2048]{1,0:T(8,128)(2,1)S(1)} all-gather(bf16[32,128]{1,0:T(8,128)(2,1)S(1)} %get-tuple-element.24), channel_id=1, replica_groups=mesh['tp'=16,'dp'=2] {'tp'}, dimensions={1}, use_global_device_ids=true | all-gather | bytes 139264 | tf_op jit(solution)/shard_map/all_gather | solution.py:65
  263.0 19.1 %all_gather.53 = bf16[32,2048]{1,0:T(8,128)(2,1)S(1)} all-gather(bf16[32,128]{1,0:T(8,128)(2,1)S(1)} %get-tuple-element.25), channel_id=1, replica_groups=mesh['tp'=16,'dp'=2] {'tp'}, dimensions={1}, use_global_device_ids=true | all-gather | bytes 139264 | tf_op jit(solution)/shard_map/all_gather | solution.py:66
  282.1 0.1 add_bitcast_fusion
  282.3 0.2 copy.30
  282.5 2.6 fusion.2
  285.1 0.1 multiply_reduce_fusion
  285.2 57.8 %psum.15 = f32[32,16]{1,0:T(8,128)S(1)} all-reduce(f32[32,16]{1,0:T(8,128)S(1)} %multiply_reduce_fusion), channel_id=1, replica_groups=mesh['tp'=16,'dp'=2] {'tp'}, use_global_device_ids=true, to_apply=%region_8.9 | all-reduce | flops 512 | bytes 4096 | tf_op jit(solution)/shard_map/psum | solution.py:78
  343.0 0.1 broadcast_multiply_fusion
  343.2 0.2 copy.31
  343.4 1.0 convolution_bitcast_fusion
  344.4 3.5 multiply_add_fusion.1
  348.0 2.3 pad_maximum_fusion
  350.2 47.3 %reduce-scatter.5.cloned.1.call-done = f32[128,32]{0,1:T(8,128)} async-done(((f32[2048,32]{0,1:T(8,128)}), f32[128,32]{0,1:T(8,128)}) %reduce-scatter.5.cloned.1.call-update) | async-done | bytes 16400 | tf_op jit(solution)/shard_map/reduce_scatter | solution.py:86
  397.5 1.3 fusion.46
  (41 shorter events, 0.8 us)
Async XLA Ops:
  7.2 35.5 %copy-start.3 = (bf16[2,1024,128]{2,1,0:T(8,128)(2,1)S(1)}, bf16[2,1024,128]{2,1,0:T(8,128)(2,1)}, u32[]{:S(2)}) copy-start(bf16[2,1024,128]{2,1,0:T(8,128)(2,1)} %param.13) | copy-start | bytes 1572868
  7.2 212.8 %reduce-scatter.3.cloned.1.call-start = ((), (), s32[]{:S(2)}) async-start(), calls=%async_computation.2 | async-start | bytes 278528 | tf_op jit(solution)/shard_map/reduce_scatter | solution.py:86
  32.8 18.8 %copy-start.4 = (bf16[2,1024,16,8]{1,3,2,0:T(8,128)(2,1)S(1)}, bf16[2,1024,16,8]{1,3,2,0:T(8,128)(2,1)}, u32[]{:S(2)}) copy-start(bf16[2,1024,16,8]{1,3,2,0:T(8,128)(2,1)} %param.14) | copy-start | bytes 1572868
  42.7 16.8 %copy-start.5 = (bf16[2,1024,16,8]{1,3,2,0:T(8,128)(2,1)S(1)}, bf16[2,1024,16,8]{1,3,2,0:T(8,128)(2,1)}, u32[]{:S(2)}) copy-start(bf16[2,1024,16,8]{1,3,2,0:T(8,128)(2,1)} %param.15) | copy-start | bytes 1572868
  51.6 15.4 %copy-start.8 = (f32[2,16,8]{1,2,0:T(8,128)S(1)}, f32[2,16,8]{1,2,0:T(8,128)}, u32[]{:S(2)}) copy-start(f32[2,16,8]{1,2,0:T(8,128)} %param.18) | copy-start | bytes 3076
  51.6 15.6 %copy-start.7 = (f32[2,2048]{1,0:T(2,128)S(1)}, f32[2,2048]{1,0:T(2,128)}, u32[]{:S(2)}) copy-start(f32[2,2048]{1,0:T(2,128)} %param.16) | copy-start | bytes 49156
  104.8 61.0 %copy-start = (bf16[2,16,8,2048]{3,2,1,0:T(8,128)(2,1)S(1)}, bf16[2,16,8,2048]{3,2,1,0:T(8,128)(2,1)}, u32[]{:S(2)}) copy-start(bf16[2,16,8,2048]{3,2,1,0:T(8,128)(2,1)} %param.19) | copy-start | bytes 3145732
  165.8 54.2 %copy-start.6 = (bf16[32,128]{1,0:T(8,128)(2,1)S(1)}, bf16[32,128]{1,0:T(8,128)(2,1)}, u32[]{:S(2)}) copy-start(bf16[32,128]{1,0:T(8,128)(2,1)} %param.10) | copy-start | bytes 24580
  166.8 230.7 %reduce-scatter.5.cloned.1.call-start = ((), (), s32[]{:S(2)}) async-start(), calls=%async_computation.3 | async-start | bytes 278528 | tf_op jit(solution)/shard_map/reduce_scatter | solution.py:86
  185.7 58.9 %copy-start.1 = (bf16[1,2048,128]{2,1,0:T(8,128)(2,1)S(1)}, bf16[1,2048,128]{2,1,0:T(8,128)(2,1)}, u32[]{:S(2)}) copy-start(bf16[1,2048,128]{2,1,0:T(8,128)(2,1)} %all-gather.2) | copy-start | bytes 1572868
  201.3 43.1 %copy-start.2 = (bf16[2048,128]{0,1:T(8,128)(2,1)S(1)}, bf16[2048,128]{0,1:T(8,128)(2,1)}, u32[]{:S(2)}) copy-start(bf16[2048,128]{0,1:T(8,128)(2,1)} %all_gather.55) | copy-start | bytes 1572868
Sparse Core Ops, SparseCore 0:
  166.9 52.9 reduce-scatter.2
  344.5 52.9 reduce-scatter.4
where the time goes:
time: 406 us
  blocking collectives  300 us (74%)
  waiting for transfers between devices  66 us (16%)
  other arithmetic  14.4 us (4%)
  between operations  14.4 us (4%)
  matrix products  7.68 us (2%)
    psum x2, blocking collectives, shards(): power_sum = lax.psum(jnp.sum(readout * readout, axis=2), 'tp')  116 us
    reduce_scatter x2, waiting for transfers between devices, shards(): lax.psum_scatter(lax.dot_general(weight_out, flattened, (((0,), (1,)), ((...  66 us
    all_gather x2, blocking collectives, shards(): gathered = lax.all_gather(residual, 'tp', axis=1, tiled=True)  43.5 us
    all_gather x2, blocking collectives, shards(): lax.all_gather(forget_pre, 'tp', axis=1, tiled=True)  38.5 us
    all_gather x2, blocking collectives, shards(): lax.all_gather(queries, 'tp', axis=1, tiled=True)  35.3 us
    all_gather x2, blocking collectives, shards(): lax.all_gather(query_rows, 'dp', axis=0, tiled=True)  18.8 us
    all_gather x2, blocking collectives, shards(): lax.all_gather(forget_rows, 'dp', axis=0, tiled=True)  17.7 us
    all_gather x2, blocking collectives, shards(): lax.all_gather(value_rows, 'dp', axis=0, tiled=True)  15.9 us
  transfers between devices with their start and end apart: 2, of which 2 were waited for; matrix products, arithmetic and copies ran while one was open for 1% of the time, Pallas kernels for 0%

commit v1 on v0

v1 whole, which is shorter than its diff:
```python
import jax
import jax.numpy as jnp
from jax import lax
from jax.sharding import PartitionSpec as P

BLOCKS = 2


epsilon = 1e-06


def gather_tp(piece, tp_size):
    copies = jnp.broadcast_to(piece[None], (tp_size,) + piece.shape)
    return lax.all_to_all(copies, "tp", 0, 0, tiled=True)


def shards(
    tp_size, dp_size,
    resid, norm_gain, w_query, w_forget, w_value, w_gate, gate_floor, states, out_gain, w_out
):
    seq_local, feat_local = resid.shape
    heads, slice_cols, head_dim = states.shape[2:]
    row_count = w_query.shape[1]
    dp_here = lax.axis_index("dp")

    weights = []
    for layer in range(BLOCKS):
        keys_own = jnp.stack([w_query[layer], w_forget[layer]])
        values_own = jnp.stack([w_value[layer], w_gate[layer]])
        parts = [(keys_own, values_own)]
        for k in range(1, dp_size):
            pairs = [(i, (i - k) % dp_size) for i in range(dp_size)]
            parts.append((lax.ppermute(keys_own, "dp", pairs), lax.ppermute(values_own, "dp", pairs)))
        weights.append(parts)

    residual = resid
    new_list = []
    for layer in range(BLOCKS):
        gathered = gather_tp(residual, tp_size)
        resid_f32 = gathered.astype(jnp.float32)
        inv_rms = lax.rsqrt(jnp.mean(resid_f32 * resid_f32, axis=(0, 2)) + epsilon)[:, None]
        gain = norm_gain[layer].reshape(tp_size, 1, feat_local)
        scaled = (resid_f32 * gain).astype(jnp.bfloat16)
        scaled = scaled.transpose(1, 0, 2).reshape(seq_local, -1)
        totals = [0.0, 0.0, 0.0, 0.0]
        for k in range(dp_size):
            lo_row = ((dp_here + k) % dp_size) * row_count
            columns = lax.dynamic_slice_in_dim(scaled, lo_row, row_count, 1)
            keys_k, values_k = weights[layer][k]
            mats = (keys_k[0], keys_k[1], values_k[0].reshape(row_count, -1), values_k[1].reshape(row_count, -1))
            totals = [
                total
                + lax.optimization_barrier(
                    jnp.dot(columns, mat, preferred_element_type=jnp.float32).astype(jnp.bfloat16)
                ).astype(jnp.float32)
                for total, mat in zip(totals, mats)
            ]
        queries, forget_pre, values, gate_pre = [
            (summed * inv_rms).astype(jnp.bfloat16) for summed in totals
        ]
        pair_all = gather_tp(jnp.concatenate([queries, forget_pre], axis=1), tp_size)
        pair_all = pair_all.astype(jnp.float32)
        query_all = pair_all[:, :, : queries.shape[1]].transpose(1, 0, 2).reshape(seq_local, heads, head_dim)
        forget_all = pair_all[:, :, queries.shape[1] :].transpose(1, 0, 2).reshape(seq_local, heads, head_dim)
        floor_now = gate_floor[layer].reshape(heads, head_dim)
        keep = floor_now + (1.0 - floor_now) * jax.nn.sigmoid(forget_all)
        value_f32 = values.astype(jnp.float32).reshape(seq_local, heads, slice_cols)
        state_new = (
            keep[:, :, None, :] * states[layer]
            + (1.0 - keep)[:, :, None, :] * value_f32[:, :, :, None]
        )
        readout = jnp.sum(query_all[:, :, None, :] * state_new, axis=3)
        power_sum = gather_tp(jnp.sum(readout * readout, axis=2), tp_size).sum(axis=0)
        mean_square = power_sum[..., None] / head_dim
        gate_f32 = gate_pre.astype(jnp.float32).reshape(seq_local, heads, slice_cols)
        normed = (
            readout * lax.rsqrt(mean_square + epsilon) * out_gain[layer] * jax.nn.silu(gate_f32)
        ).astype(jnp.bfloat16)
        flattened = normed.reshape(seq_local, heads * slice_cols)
        weight_out = w_out[layer].reshape(heads * slice_cols, -1)
        branch = jnp.dot(flattened, weight_out, preferred_element_type=jnp.float32).astype(jnp.bfloat16)
        branch = branch.reshape(seq_local, tp_size, feat_local).transpose(1, 0, 2)
        terms = lax.all_to_all(branch, "tp", 0, 0, tiled=True)
        residual = (
            residual.astype(jnp.float32) + terms.astype(jnp.float32).sum(axis=0)
        ).astype(jnp.bfloat16)
        new_list.append(state_new)
    return (residual, jnp.stack(new_list))


def solution(mesh):
    tp_size, dp_size = mesh.shape["tp"], mesh.shape["dp"]

    def body(*args):
        return shards(tp_size, dp_size, *args)

    return jax.shard_map(
        body,
        mesh=mesh,
        in_specs=(
            P("dp", "tp"),
            P(),
            P(None, "dp", "tp"),
            P(None, "dp", "tp"),
            P(None, "dp", None, "tp"),
            P(None, "dp", None, "tp"),
            P(),
            P(None, "dp", None, "tp", None),
            P(None, None, "tp"),
            P(None, None, "tp", None),
        ),
        out_specs=(P("dp", "tp"), P(None, "dp", None, "tp", None)),
        check_vma=False,
    )
```

time: 406 us -> 162 us (0.40)
  blocking collectives: 300 us -> 10.5 us
  starting transfers between devices: 0.08 us -> 37 us
  between operations: 14.4 us -> 1.17 us
  local copies, waits for them, and re-layouts: 3.55 us -> 14.8 us
  other arithmetic: 14.4 us -> 20.4 us
    all_gather x14 -> x0, blocking collectives: 184 us -> none  [the longest x2 43.5 us: shards(): gathered = lax.all_gather(residual, 'tp', axis=1, tiled=True)]
    psum x2 -> x0, blocking collectives: 116 us -> none  [shards(): power_sum = lax.psum(jnp.sum(readout * readout, axis=2), 'tp')]
    reduce_scatter x2 -> x0, waiting for transfers between devices: 66 us -> none  [shards(): lax.psum_scatter(lax.dot_general(weight_out, flattened, (((0,), (1,)), ((...]
    all_to_all x0 -> x7, waiting for transfers between devices: none -> 33 us  [the longest x6 30.9 us: gather_tp(): return lax.all_to_all(copies, 'tp', 0, 0, tiled=True)]
    all_to_all x0 -> x7, starting transfers between devices: none -> 32.9 us  [the longest x6 29.4 us: gather_tp(): return lax.all_to_all(copies, 'tp', 0, 0, tiled=True)]
    ppermute x0 -> x4, waiting for transfers between devices: none -> 32.7 us  [the longest x2 16.5 us: shards(): lax.ppermute(values_own, 'dp', pairs)]
    all_to_all x0 -> x1, blocking collectives: none -> 10.5 us  [shards(): terms = lax.all_to_all(branch, 'tp', 0, 0, tiled=True)]
    another operation x0 -> x4, other arithmetic: none -> 4.64 us  [the longest x2 2.71 us: shards(): values_own = jnp.stack([w_value[layer], w_gate[layer]])]
  transfers between devices with their start and end apart: 2 -> 11, of which waited for: 2 -> 11; matrix products, arithmetic and copies ran while one was open for 1% -> 16% of each run, Pallas kernels for 0% -> 0%
where the time goes in v1:
time: 162 us; the launch traced here: 161 us
  waiting for transfers between devices  65.6 us (40%)
  starting transfers between devices  37 us (23%)
  other arithmetic  20.4 us (13%)
  local copies, waits for them, and re-layouts  14.8 us (9%)
  matrix products  11.4 us (7%)
  blocking collectives  10.5 us (6%)
    all_to_all x6, waiting for transfers between devices, gather_tp(): return lax.all_to_all(copies, 'tp', 0, 0, tiled=True)  30.9 us
    all_to_all x6, starting transfers between devices, gather_tp(): return lax.all_to_all(copies, 'tp', 0, 0, tiled=True)  29.4 us
    ppermute x2, waiting for transfers between devices, shards(): lax.ppermute(values_own, 'dp', pairs)  16.5 us
    ppermute x2, waiting for transfers between devices, shards(): lax.ppermute(keys_own, 'dp', pairs)  16.1 us
    all_to_all x1, blocking collectives, shards(): terms = lax.all_to_all(branch, 'tp', 0, 0, tiled=True)  10.5 us
    dot_general x16, matrix products, shards(): jnp.dot(columns, mat, preferred_element_type=jnp.float32)  8.68 us
    reduce_sum x2, other arithmetic, shards(): readout = jnp.sum(query_all[:, :, None, :] * state_new, axis=3)  5.17 us
    broadcast_in_dim x4, local copies, waits for them, and re-layouts, gather_tp(): copies = jnp.broadcast_to(piece[None], (tp_size,) + piece.shape)  3.58 us
  transfers between devices with their start and end apart: 11, of which 11 were waited for; matrix products, arithmetic and copies ran while one was open for 16% of the time, Pallas kernels for 0%

profile of v1, /device:TPU:0, one launch (start us, length us, event | category | flops | bytes accessed | tf_op | source)
XLA Modules:
  0.0 160.9 jit_solution(7711456989257921505)
XLA Ops:
  0.6 1.5 broadcast_in_dim.12
  2.1 7.4 %all-to-all-start = ((bf16[16,32,128]{2,1,0:T(8,128)(2,1)}), bf16[16,32,128]{2,1,0:T(8,128)(2,1)S(1)}, u32[]{:S(2)}, u32[]{:S(2)}) async-start(bf16[16,32,128]{2,1,0:T(8,128)(2,1)} %broadcast_in_dim.12), calls=%async_computation | async-start | bytes 262144 | tf_op jit(solution)/shard_map/all_to_all | solution.py:14
  9.5 2.1 %fusion.102 = (bf16[1,1024,128]{2,1,0:T(8,128)(2,1)}, bf16[1,1024,128]{2,1,0:T(8,128)(2,1)S(1)}, bf16[1,1024,128]{2,1,0:T(8,128)(2,1)S(1)}, bf16[1,1024,128]{2,1,0:T(8,128)(2,1)}) fusion(bf16[2,1024,128]{2,1,0:T(8,128)(2,1)} %param.12, bf16[2,1024,128]{2,1,0:T(8,128)(2,1)} %param.13), kind=kLoop, calls=%fused_computation.175 | loop fusion | bytes 2097152 | tf_op jit(solution)/shard_map/slice | solution.py:28
  11.7 1.6 collective-permute-start
  13.2 0.9 fusion.104
  14.1 0.8 pad_maximum_fusion.2
  14.9 0.5 collective-permute-start.1
  15.5 0.6 fusion.107
  16.1 0.8 fusion.106
  16.9 0.5 all-to-all-done
  17.8 0.2 convolution_convert_fusion.13
  18.2 8.4 %collective-permute-done = bf16[2,1024,128]{2,1,0:T(8,128)(2,1)} collective-permute-done((bf16[2,1024,128]{2,1,0:T(8,128)(2,1)S(1)}, bf16[2,1024,128]{2,1,0:T(8,128)(2,1)}, u32[]{:S(2)}, u32[]{:S(2)}) %collective-permute-start) | collective-permute-done | bytes 524320 | tf_op jit(solution)/shard_map/ppermute | solution.py:33
  26.6 1.1 convolution_convert_fusion.16
  27.7 1.1 convolution_convert_fusion.14
  28.9 8.3 %collective-permute-done.1 = bf16[2,1024,16,8]{1,3,2,0:T(8,128)(2,1)S(1)} collective-permute-done((bf16[2,1024,16,8]{1,3,2,0:T(8,128)(2,1)}, bf16[2,1024,16,8]{1,3,2,0:T(8,128)(2,1)S(1)}, u32[]{:S(2)}, u32[]{:S(2)}) %collective-permute-start.1) | collective-permute-done | bytes 524320 | tf_op jit(solution)/shard_map/ppermute | solution.py:33
  37.2 0.2 convolution_convert_fusion.12
  37.5 0.7 broadcast_in_dim.13
  38.2 5.7 %all-to-all-start.1 = ((bf16[16,32,256]{2,1,0:T(8,128)(2,1)}), bf16[16,32,256]{2,1,0:T(8,128)(2,1)S(1)}, u32[]{:S(2)}, u32[]{:S(2)}) async-start(bf16[16,32,256]{2,1,0:T(8,128)(2,1)} %broadcast_in_dim.13), calls=%async_computation.1 | async-start | bytes 524288 | tf_op jit(solution)/shard_map/all_to_all | solution.py:14
  43.9 0.6 fusion.108
  44.6 0.6 mul.300
  45.2 0.8 convolution_convert_fusion.11
  46.3 7.7 %all-to-all-done.1 = bf16[16,32,256]{2,1,0:T(8,128)(2,1)S(1)} async-done(((bf16[16,32,256]{2,1,0:T(8,128)(2,1)}), bf16[16,32,256]{2,1,0:T(8,128)(2,1)S(1)}, u32[]{:S(2)}, u32[]{:S(2)}) %all-to-all-start.1) | async-done | bytes 262176 | tf_op jit(solution)/shard_map/all_to_all | solution.py:14
  54.6 2.6 %fusion.5 = f32[32,16,8]{2,1,0:T(8,128)S(1)} fusion(f32[2,32,16,8,128]{4,3,2,1,0:T(8,128)} %param.17, f32[32,16,8]{2,1,0:T(8,128)S(1)} %copy.87, f32[32,16,128]{2,1,0:T(8,128)S(1)} %copy.85, f32[32,16,128]{2,1,0:T(8,128)S(1)} %copy.84, f32[32,16,128]{2,1,0:T(8,128)S(1)} %copy.83), kind=kLoop, calls=%fused_computation.10 | loop fusion | flops 2617344 | bytes 2916352 | tf_op jit(solution)/shard_map/reduce_sum | solution.py:72
  57.4 0.7 reshape.96
  58.2 3.5 %all-to-all-start.2 = ((f32[16,1,512]{2,1,0:T(1,128)}), f32[16,1,512]{2,1,0:T(1,128)S(1)}, u32[]{:S(2)}, u32[]{:S(2)}) async-start(f32[16,1,512]{2,1,0:T(1,128)} %reshape.96), calls=%async_computation.2 | async-start | bytes 65536 | tf_op jit(solution)/shard_map/all_to_all | solution.py:14
  61.7 1.8 %convolution_convert_fusion.10 = bf16[32,128]{1,0:T(8,128)(2,1)} fusion(bf16[2,1024,16,8]{1,3,2,0:T(8,128)(2,1)} %copy-done.4, bf16[32,2048]{1,0:T(8,128)(2,1)S(1)} %bitcast.139, s32[]{:T(128)S(6)} %select_n.26), kind=kOutput, calls=%fused_computation.23 | convolution fusion | flops 8392704 | bytes 335876 | tf_op jit(solution)/shard_map/dot_general | solution.py:54
  63.4 4.8 %all-to-all-done.2 = f32[16,1,512]{2,1,0:T(1,128)S(1)} async-done(((f32[16,1,512]{2,1,0:T(1,128)}), f32[16,1,512]{2,1,0:T(1,128)S(1)}, u32[]{:S(2)}, u32[]{:S(2)}) %all-to-all-start.2) | async-done | bytes 32800 | tf_op jit(solution)/shard_map/all_to_all | solution.py:14
  68.2 0.6 broadcast.164
  68.8 0.8 reduce
  70.2 1.4 fusion.6
  71.6 10.5 %all_to_all.40 = bf16[16,32,128]{2,1,0:T(8,128)(2,1)S(1)} all-to-all(bf16[16,32,128]{2,1,0:T(8,128)(2,1)S(1)} %bitcast.140), channel_id=1, replica_groups=mesh['tp'=16,'dp'=2] {'tp'}, dimensions={0} | all-to-all | bytes 262144 | tf_op jit(solution)/shard_map/all_to_all | solution.py:83
  82.1 0.7 add_convert_fusion.1
  82.8 0.7 broadcast_in_dim.15
  83.5 3.5 %all-to-all-start.4 = ((bf16[16,32,128]{2,1,0:T(8,128)(2,1)}), bf16[16,32,128]{2,1,0:T(8,128)(2,1)S(1)}, u32[]{:S(2)}, u32[]{:S(2)}) async-start(bf16[16,32,128]{2,1,0:T(8,128)(2,1)} %broadcast_in_dim.15), calls=%async_computation.4 | async-start | bytes 262144 | tf_op jit(solution)/shard_map/all_to_all | solution.py:14
  87.0 1.9 %pad_maximum_fusion.3 = bf16[2,1024,128]{2,1,0:T(8,128)(2,1)} fusion(bf16[1,1024,128]{2,1,0:T(8,128)(2,1)} %get-tuple-element.33, bf16[1,1024,128]{2,1,0:T(8,128)(2,1)} %get-tuple-element.8), kind=kLoop, calls=%fused_computation.33 | loop fusion | flops 262144 | bytes 1048576 | tf_op jit(solution)/shard_map/stack | solution.py:28
  88.9 1.5 collective-permute-start.2
  90.4 1.9 %pad_maximum_fusion.4 = bf16[2,1024,16,8]{1,3,2,0:T(8,128)(2,1)} fusion(bf16[1,1024,16,8]{1,3,2,0:T(8,128)(2,1)} %get-tuple-element.34, bf16[1,1024,16,8]{1,3,2,0:T(8,128)(2,1)} %get-tuple-element.13), kind=kLoop, calls=%fused_computation.34 | loop fusion | flops 262144 | bytes 1048576 | tf_op jit(solution)/shard_map/stack | solution.py:29
  92.2 0.5 collective-permute-start.3
  92.8 2.1 %all-to-all-done.4 = bf16[16,32,128]{2,1,0:T(8,128)(2,1)S(1)} async-done(((bf16[16,32,128]{2,1,0:T(8,128)(2,1)}), bf16[16,32,128]{2,1,0:T(8,128)(2,1)S(1)}, u32[]{:S(2)}, u32[]{:S(2)}) %all-to-all-start.4) | async-done | bytes 131104 | tf_op jit(solution)/shard_map/all_to_all | solution.py:14
  94.9 0.9 fusion.15
  95.9 0.2 convolution_convert_fusion.5
  96.1 0.2 convolution_convert_fusion.9
  96.3 7.7 %collective-permute-done.2 = bf16[2,1024,128]{2,1,0:T(8,128)(2,1)} collective-permute-done((bf16[2,1024,128]{2,1,0:T(8,128)(2,1)}, bf16[2,1024,128]{2,1,0:T(8,128)(2,1)}, u32[]{:S(2)}, u32[]{:S(2)}) %collective-permute-start.2) | collective-permute-done | bytes 524320 | tf_op jit(solution)/shard_map/ppermute | solution.py:33
  104.0 1.1 convolution_convert_fusion.8
  105.1 1.1 convolution_convert_fusion.6
  106.2 8.2 %collective-permute-done.3 = bf16[2,1024,16,8]{1,3,2,0:T(8,128)(2,1)S(1)} collective-permute-done((bf16[2,1024,16,8]{1,3,2,0:T(8,128)(2,1)}, bf16[2,1024,16,8]{1,3,2,0:T(8,128)(2,1)S(1)}, u32[]{:S(2)}, u32[]{:S(2)}) %collective-permute-start.3) | collective-permute-done | bytes 524320 | tf_op jit(solution)/shard_map/ppermute | solution.py:33
  114.4 0.2 convolution_convert_fusion.4
  114.7 0.7 broadcast_in_dim.16
  115.4 5.8 %all-to-all-start.5 = ((bf16[16,32,256]{2,1,0:T(8,128)(2,1)}), bf16[16,32,256]{2,1,0:T(8,128)(2,1)S(1)}, u32[]{:S(2)}, u32[]{:S(2)}) async-start(bf16[16,32,256]{2,1,0:T(8,128)(2,1)} %broadcast_in_dim.16), calls=%async_computation.5 | async-start | bytes 524288 | tf_op jit(solution)/shard_map/all_to_all | solution.py:14
  121.7 0.2 convolution_convert_fusion.3
  121.9 9.4 %all-to-all-done.5 = bf16[16,32,256]{2,1,0:T(8,128)(2,1)S(1)} async-done(((bf16[16,32,256]{2,1,0:T(8,128)(2,1)}), bf16[16,32,256]{2,1,0:T(8,128)(2,1)S(1)}, u32[]{:S(2)}, u32[]{:S(2)}) %all-to-all-start.5) | async-done | bytes 262176 | tf_op jit(solution)/shard_map/all_to_all | solution.py:14
  131.9 2.6 %fusion.2 = f32[32,16,8]{2,1,0:T(8,128)S(1)} fusion(f32[2,32,16,8,128]{4,3,2,1,0:T(8,128)} %param.17, f32[32,16,8]{2,1,0:T(8,128)S(1)} %copy.100, f32[32,16,128]{2,1,0:T(8,128)S(1)} %copy.98, f32[32,16,128]{2,1,0:T(8,128)S(1)} %copy.97, f32[32,16,128]{2,1,0:T(8,128)S(1)} %copy.96), kind=kLoop, calls=%fused_computation.6 | loop fusion | flops 2617344 | bytes 2916352 | tf_op jit(solution)/shard_map/reduce_sum | solution.py:72
  134.7 0.7 reshape.98
  135.4 3.5 %all-to-all-start.6 = ((f32[16,1,512]{2,1,0:T(1,128)}), f32[16,1,512]{2,1,0:T(1,128)S(1)}, u32[]{:S(2)}, u32[]{:S(2)}) async-start(f32[16,1,512]{2,1,0:T(1,128)} %reshape.98), calls=%async_computation.6 | async-start | bytes 65536 | tf_op jit(solution)/shard_map/all_to_all | solution.py:14
  138.9 0.2 convolution_convert_fusion.2
  139.1 6.4 %all-to-all-done.6 = f32[16,1,512]{2,1,0:T(1,128)S(1)} async-done(((f32[16,1,512]{2,1,0:T(1,128)}), f32[16,1,512]{2,1,0:T(1,128)S(1)}, u32[]{:S(2)}, u32[]{:S(2)}) %all-to-all-start.6) | async-done | bytes 32800 | tf_op jit(solution)/shard_map/all_to_all | solution.py:14
  145.5 0.8 reduce.1
  146.9 1.3 fusion.7
  148.2 0.7 copy.124
  148.9 3.5 %all-to-all-start.7 = ((bf16[16,32,128]{2,1,0:T(8,128)(2,1)}), bf16[16,32,128]{2,1,0:T(8,128)(2,1)S(1)}, u32[]{:S(2)}, u32[]{:S(2)}) async-start(bf16[16,32,128]{2,1,0:T(8,128)(2,1)} %bitcast.121), calls=%async_computation.7 | async-start | bytes 262144 | tf_op jit(solution)/shard_map/all_to_all | solution.py:83
  152.4 3.5 %multiply_add_fusion.1 = (f32[1,32,16,8,128]{4,3,2,1,0:T(8,128)S(1)}, f32[1,32,16,8,128]{4,3,2,1,0:T(8,128)S(1)}) fusion(f32[2,32,16,8,128]{4,3,2,1,0:T(8,128)} %param.17, f32[32,16,8]{2,1,0:T(8,128)S(1)} %copy.87, f32[32,16,128]{2,1,0:T(8,128)S(1)} %copy.85, f32[32,16,128]{2,1,0:T(8,128)S(1)} %copy.84, f32[32,16,8]{2,1,0:T(8,128)S(1)} %copy.100, ...), kind=kLoop, calls=%fused_computation.12 | loop fusion | flops 3145728 | bytes 9469952 | tf_op jit(solution)/shard_map/add | solution.py:69
  155.9 2.3 %pad_maximum_fusion = f32[2,32,16,8,128]{4,3,2,1,0:T(8,128)} fusion(f32[1,32,16,8,128]{4,3,2,1,0:T(8,128)S(1)} %get-tuple-element.7, f32[1,32,16,8,128]{4,3,2,1,0:T(8,128)S(1)} %get-tuple-element.6), kind=kLoop, calls=%fused_computation | loop fusion | flops 1048576 | bytes 8388608 | tf_op jit(solution)/shard_map/stack | solution.py:88
  158.2 2.1 %all-to-all-done.7 = bf16[16,32,128]{2,1,0:T(8,128)(2,1)S(1)} async-done(((bf16[16,32,128]{2,1,0:T(8,128)(2,1)}), bf16[16,32,128]{2,1,0:T(8,128)(2,1)S(1)}, u32[]{:S(2)}, u32[]{:S(2)}) %all-to-all-start.7) | async-done | bytes 131104 | tf_op jit(solution)/shard_map/all_to_all | solution.py:83
  160.3 0.6 add_convert_fusion
  (77 shorter events, 4.5 us)
Async XLA Ops:
  0.6 12.6 %copy-start.3 = (bf16[2,1024,16,8]{1,3,2,0:T(8,128)(2,1)S(1)}, bf16[2,1024,16,8]{1,3,2,0:T(8,128)(2,1)}, u32[]{:S(2)}) copy-start(bf16[2,1024,16,8]{1,3,2,0:T(8,128)(2,1)} %param.15) | copy-start | bytes 1572868
  0.6 12.6 %copy-start.1 = (bf16[2,1024,16,8]{1,3,2,0:T(8,128)(2,1)S(1)}, bf16[2,1024,16,8]{1,3,2,0:T(8,128)(2,1)}, u32[]{:S(2)}) copy-start(bf16[2,1024,16,8]{1,3,2,0:T(8,128)(2,1)} %param.14) | copy-start | bytes 1572868
  2.1 15.3 %all-to-all-start = ((bf16[16,32,128]{2,1,0:T(8,128)(2,1)}), bf16[16,32,128]{2,1,0:T(8,128)(2,1)S(1)}, u32[]{:S(2)}, u32[]{:S(2)}) async-start(bf16[16,32,128]{2,1,0:T(8,128)(2,1)} %broadcast_in_dim.12), calls=%async_computation | async-start | bytes 262144 | tf_op jit(solution)/shard_map/all_to_all | solution.py:14
  11.6 3.9 %copy-start.6 = (f32[2,2048]{1,0:T(2,128)S(1)}, f32[2,2048]{1,0:T(2,128)}, u32[]{:S(2)}) copy-start(f32[2,2048]{1,0:T(2,128)} %param.11) | copy-start | bytes 49156
  11.6 6.0 %copy-start = (bf16[2,1024,128]{2,1,0:T(8,128)(2,1)S(1)}, bf16[2,1024,128]{2,1,0:T(8,128)(2,1)}, u32[]{:S(2)}) copy-start(bf16[2,1024,128]{2,1,0:T(8,128)(2,1)} %param.13) | copy-start | bytes 1572868
  11.7 6.3 %copy-start.2 = (bf16[2,1024,128]{2,1,0:T(8,128)(2,1)S(1)}, bf16[2,1024,128]{2,1,0:T(8,128)(2,1)}, u32[]{:S(2)}) copy-start(bf16[2,1024,128]{2,1,0:T(8,128)(2,1)} %param.12) | copy-start | bytes 1572868
  11.7 15.0 %collective-permute-start = (bf16[2,1024,128]{2,1,0:T(8,128)(2,1)S(1)}, bf16[2,1024,128]{2,1,0:T(8,128)(2,1)}, u32[]{:S(2)}, u32[]{:S(2)}) collective-permute-start(bf16[2,1024,128]{2,1,0:T(8,128)(2,1)S(1)} %pad_maximum_fusion.1), channel_id=1, source_target_pairs={{0,1},{1,0},{2,3},{3,2},{4,5},{5,4},{6,7},{7,6},{8,9},{9,8},{10,11... | collective-permute-start | bytes 1572872 | tf_op jit(solution)/shard_map/ppermute | solution.py:33
  14.9 29.0 %copy-start.8 = (f32[2,16,8]{1,2,0:T(8,128)S(1)}, f32[2,16,8]{1,2,0:T(8,128)}, u32[]{:S(2)}) copy-start(f32[2,16,8]{1,2,0:T(8,128)} %param.18) | copy-start | bytes 3076
  14.9 22.3 %collective-permute-start.1 = (bf16[2,1024,16,8]{1,3,2,0:T(8,128)(2,1)}, bf16[2,1024,16,8]{1,3,2,0:T(8,128)(2,1)S(1)}, u32[]{:S(2)}, u32[]{:S(2)}) collective-permute-start(bf16[2,1024,16,8]{1,3,2,0:T(8,128)(2,1)} %pad_maximum_fusion.2), channel_id=1, source_target_pairs={{0,1},{1,0},{2,3},{3,2},{4,5},{5,4},{6,7},{7,6},{8,9},{9,8},{10,11... | collective-permute-start | bytes 1572872 | tf_op jit(solution)/shard_map/ppermute | solution.py:33
  18.2 27.9 %copy-start.9 = (f32[32]{0:T(128)}, f32[32]{0:T(128)S(1)}, u32[]{:S(2)}) copy-start(f32[32]{0:T(128)S(1)} %add_rsqrt_fusion.3) | copy-start | bytes 388
  37.2 1.0 copy-start.4
  38.2 15.7 %all-to-all-start.1 = ((bf16[16,32,256]{2,1,0:T(8,128)(2,1)}), bf16[16,32,256]{2,1,0:T(8,128)(2,1)S(1)}, u32[]{:S(2)}, u32[]{:S(2)}) async-start(bf16[16,32,256]{2,1,0:T(8,128)(2,1)} %broadcast_in_dim.13), calls=%async_computation.1 | async-start | bytes 524288 | tf_op jit(solution)/shard_map/all_to_all | solution.py:14
  54.6 15.6 %copy-start.5 = (bf16[32,128]{1,0:T(8,128)(2,1)S(1)}, bf16[32,128]{1,0:T(8,128)(2,1)}, u32[]{:S(2)}) copy-start(bf16[32,128]{1,0:T(8,128)(2,1)} %convolution_convert_fusion.11) | copy-start | bytes 24580
  58.2 10.1 %all-to-all-start.2 = ((f32[16,1,512]{2,1,0:T(1,128)}), f32[16,1,512]{2,1,0:T(1,128)S(1)}, u32[]{:S(2)}, u32[]{:S(2)}) async-start(f32[16,1,512]{2,1,0:T(1,128)} %reshape.96), calls=%async_computation.2 | async-start | bytes 65536 | tf_op jit(solution)/shard_map/all_to_all | solution.py:14
  83.5 11.4 %all-to-all-start.4 = ((bf16[16,32,128]{2,1,0:T(8,128)(2,1)}), bf16[16,32,128]{2,1,0:T(8,128)(2,1)S(1)}, u32[]{:S(2)}, u32[]{:S(2)}) async-start(bf16[16,32,128]{2,1,0:T(8,128)(2,1)} %broadcast_in_dim.15), calls=%async_computation.4 | async-start | bytes 262144 | tf_op jit(solution)/shard_map/all_to_all | solution.py:14
  88.9 15.1 %collective-permute-start.2 = (bf16[2,1024,128]{2,1,0:T(8,128)(2,1)}, bf16[2,1024,128]{2,1,0:T(8,128)(2,1)}, u32[]{:S(2)}, u32[]{:S(2)}) collective-permute-start(bf16[2,1024,128]{2,1,0:T(8,128)(2,1)} %pad_maximum_fusion.3), channel_id=1, source_target_pairs={{0,1},{1,0},{2,3},{3,2},{4,5},{5,4},{6,7},{7,6},{8,9},{9,8},{10,11... | collective-permute-start | bytes 1572872 | tf_op jit(solution)/shard_map/ppermute | solution.py:33
  92.2 22.2 %collective-permute-start.3 = (bf16[2,1024,16,8]{1,3,2,0:T(8,128)(2,1)}, bf16[2,1024,16,8]{1,3,2,0:T(8,128)(2,1)S(1)}, u32[]{:S(2)}, u32[]{:S(2)}) collective-permute-start(bf16[2,1024,16,8]{1,3,2,0:T(8,128)(2,1)} %pad_maximum_fusion.4), channel_id=1, source_target_pairs={{0,1},{1,0},{2,3},{3,2},{4,5},{5,4},{6,7},{7,6},{8,9},{9,8},{10,11... | collective-permute-start | bytes 1572872 | tf_op jit(solution)/shard_map/ppermute | solution.py:33
  95.9 25.4 %copy-start.7 = (f32[1,16,8]{1,2,0:T(8,128)S(1)}, f32[1,16,8]{1,2,0:T(8,128)}, u32[]{:S(2)}) copy-start(f32[1,16,8]{1,2,0:T(8,128)} %get-tuple-element.24) | copy-start | bytes 1540
  115.4 15.8 %all-to-all-start.5 = ((bf16[16,32,256]{2,1,0:T(8,128)(2,1)}), bf16[16,32,256]{2,1,0:T(8,128)(2,1)S(1)}, u32[]{:S(2)}, u32[]{:S(2)}) async-start(bf16[16,32,256]{2,1,0:T(8,128)(2,1)} %broadcast_in_dim.16), calls=%async_computation.5 | async-start | bytes 524288 | tf_op jit(solution)/shard_map/all_to_all | solution.py:14
  135.4 10.1 %all-to-all-start.6 = ((f32[16,1,512]{2,1,0:T(1,128)}), f32[16,1,512]{2,1,0:T(1,128)S(1)}, u32[]{:S(2)}, u32[]{:S(2)}) async-start(f32[16,1,512]{2,1,0:T(1,128)} %reshape.98), calls=%async_computation.6 | async-start | bytes 65536 | tf_op jit(solution)/shard_map/all_to_all | solution.py:14
  148.9 11.4 %all-to-all-start.7 = ((bf16[16,32,128]{2,1,0:T(8,128)(2,1)}), bf16[16,32,128]{2,1,0:T(8,128)(2,1)S(1)}, u32[]{:S(2)}, u32[]{:S(2)}) async-start(bf16[16,32,128]{2,1,0:T(8,128)(2,1)} %bitcast.121), calls=%async_computation.7 | async-start | bytes 262144 | tf_op jit(solution)/shard_map/all_to_all | solution.py:83
